TPU v7x, 32 devices: a whole 2x2x4 slice. The times are simulated.
32 devices in a mesh: sp: 8 (over z, x), tp: 4 (over y, core).
Axes of the slice: x: 2, y: 2, z: 4, core: 2. Of those that a mesh axis runs over, the one named last changes fastest.
Arguments:
- moe_input: bfloat16 [1536, 2048], P('sp'), may hold values from -6 to 6
- out_grad: bfloat16 [1536, 2048], P('sp', 'tp'), may hold values from -6 to 6
- expert_ids: int32 [1536, 2], P('sp'), may hold values from 0 to 7, all different within a row; in each aligned block of 192 rows (0 to 191, 192 to 383, ...) at most 60 rows name the same one
- expert_weights: float32 [1536, 2], P('sp'), may hold values from 0.1 to 0.9
- w_gate: bfloat16 [8, 2048, 2048], P('sp', None, 'tp'), may hold values from -0.125 to 0.125
- w_up: bfloat16 [8, 2048, 2048], P('sp', None, 'tp'), may hold values from -0.125 to 0.125
- w_down: bfloat16 [8, 2048, 2048], P('sp', 'tp'), may hold values from -0.125 to 0.125
- out_proj: bfloat16 [1536, 2048], P('tp'), may hold values from -0.15625 to 0.15625
- retained: bfloat16 [1536, 1536], P('sp', 'tp'), may hold values from -6 to 6
- queries: bfloat16 [1536, 768], P('sp', 'tp'), may hold values from -6 to 6
- keys: bfloat16 [1536, 768], P('sp', 'tp'), may hold values from -0.86328125 to 0.86328125
- values: bfloat16 [1536, 1536], P('sp', 'tp'), may hold values from -6 to 6
- log_decay: float32 [1536, 16], P('sp', 'tp'), may hold values from -1 to 0
- incoming_state: float32 [8, 16, 48, 96], P('sp', 'tp'), may hold values from -6 to 6
Outputs:
- w_gate_grad: bfloat16 [8, 2048, 2048], P('sp', None, 'tp')
- w_up_grad: bfloat16 [8, 2048, 2048], P('sp', None, 'tp')
- w_down_grad: bfloat16 [8, 2048, 2048], P('sp', 'tp')
- out_proj_grad: float32 [2048, 1536], P('sp', 'tp')
- query_grad: bfloat16 [1536, 768], P('sp', 'tp')
- key_grad: bfloat16 [1536, 768], P('sp', 'tp')
- value_grad: bfloat16 [1536, 1536], P('sp', 'tp')
Inputs may be any that keep to these rules, and one draw needn't show every extreme that they name: `expert_ids`: in each aligned block of 192 positions no expert is named by more than 60 of the block's assignments, a bound that some block reaches.
All inputs are finite; a program needn't handle non-finite values.
Results may differ from a plain program's by a relative error of at most 0.02.
Values may be sent and summed in bfloat16 or wider, within the bound.
A program may use at most 64 MiB of HBM per device.

v0:
```python
import jax
import jax.numpy as jnp
from jax import lax
from jax.sharding import PartitionSpec as P


def carried_in(x, axis, combine, identity):
    devices, place = (lax.axis_size(axis), lax.axis_index(axis))
    everything = jax.tree.map(lambda part: lax.all_gather(part, axis), x)
    start = jax.tree.map(
        lambda part, zero: jnp.broadcast_to(jnp.asarray(zero, part.dtype), part.shape), x, identity
    )

    def lap(k, before):
        at = devices - 1 - k
        reached = at > place
        new = combine(before, jax.tree.map(lambda part: part[at], everything))
        return jax.tree.map(lambda a, b: jnp.where(reached, a, b), new, before)

    return lax.fori_loop(0, devices, lap, start)


def expert_back(rows, grad, gate_w, up_w, down_w):
    f32 = jnp.float32
    bf16 = jnp.bfloat16
    gate = jnp.dot(rows, gate_w, preferred_element_type=f32)
    up = jnp.dot(rows, up_w, preferred_element_type=f32)
    sig = jax.nn.sigmoid(gate)
    swish = gate * sig
    act = (swish * up).astype(bf16)
    across = (((1,), (1,)), ((), ()))
    along = (((0,), (0,)), ((), ()))
    act_grad = lax.dot_general(grad, down_w, across, preferred_element_type=f32)
    gate_grad = (act_grad * up * sig * (1.0 + gate * (1.0 - sig))).astype(bf16)
    up_grad = (act_grad * swish).astype(bf16)
    down_grad = lax.dot_general(act, grad, along, preferred_element_type=f32).astype(bf16)
    gate_w_grad = lax.dot_general(rows, gate_grad, along, preferred_element_type=f32).astype(bf16)
    up_w_grad = lax.dot_general(rows, up_grad, along, preferred_element_type=f32).astype(bf16)
    partial_value = lax.dot_general(
        gate_grad, gate_w, across, preferred_element_type=f32
    ) + lax.dot_general(up_grad, up_w, across, preferred_element_type=f32)
    return (gate_w_grad, up_w_grad, down_grad, partial_value)


def combine_states(earlier, later):
    return (later[0] * earlier[0], later[1] + later[0][:, None, None] * earlier[1])


def on_device(
    moe_input,
    out_grad,
    expert_ids,
    expert_weights,
    w_gate,
    w_up,
    w_down,
    out_proj,
    retained,
    queries,
    keys,
    values,
    log_decay,
    incoming_state,
):
    f32 = jnp.float32
    bf16 = jnp.bfloat16
    upper_limit = lax.Precision.HIGHEST
    tokens_here = moe_input.shape[0]
    width = moe_input.shape[1]
    sp_count = lax.axis_size("sp")
    tp_count = lax.axis_size("tp")
    capacity = 5 * tokens_here // (2 * sp_count)
    slot_count = sp_count * capacity
    flat_ids = expert_ids.reshape(-1)
    flat_weights = expert_weights.reshape(-1)
    onehot = (flat_ids[:, None] == jnp.arange(sp_count, dtype=jnp.int32)[None, :]).astype(jnp.int32)
    ranks = jnp.sum((jnp.cumsum(onehot, axis=0) - onehot) * onehot, axis=1)
    slot_of = flat_ids * capacity + ranks
    hits = jnp.arange(slot_count, dtype=jnp.int32)[:, None] == slot_of[None, :]
    picker = jnp.any(hits.reshape(slot_count, tokens_here, 2), axis=2).astype(bf16)
    slot_weight = jnp.sum(jnp.where(hits, flat_weights[None, :], 0.0), axis=1)
    along = (((0,), (0,)), ((), ()))
    column_count = width // tp_count
    own_rows = lax.dynamic_slice_in_dim(
        moe_input, lax.axis_index("tp") * column_count, column_count, 1
    )
    send_rows = jnp.dot(picker, own_rows, preferred_element_type=f32).astype(bf16)
    send_grad = (
        jnp.dot(picker, out_grad, preferred_element_type=f32) * slot_weight[:, None]
    ).astype(bf16)
    part_rows, part_grad = (
        lax.all_to_all(send_rows, "sp", split_axis=0, concat_axis=0, tiled=True),
        lax.all_to_all(send_grad, "sp", split_axis=0, concat_axis=0, tiled=True),
    )
    recv_rows, recv_grad = (
        lax.all_gather(part_rows, "tp", axis=1, tiled=True),
        lax.all_gather(part_grad, "tp", axis=1, tiled=True),
    )
    gate_w_grad, up_w_grad, down_grad, partial_value = expert_back(
        recv_rows, recv_grad, w_gate[0], w_up[0], w_down[0]
    )
    share = (
        lax.psum_scatter(partial_value.astype(jnp.bfloat16), "tp", scatter_dimension=1, tiled=True)
        .astype(jnp.float32)
        .astype(bf16)
    )
    returned = lax.all_to_all(share, "sp", split_axis=0, concat_axis=0, tiled=True)
    token_grad = lax.dot_general(picker, returned, along, preferred_element_type=f32)
    stream_part = (out_grad.astype(f32) + token_grad).astype(bf16)
    stream = lax.all_gather(stream_part, "tp", axis=1, tiled=True)
    ret_grad = lax.dot_general(
        stream, out_proj, (((1,), (1,)), ((), ())), preferred_element_type=f32
    ).astype(bf16)
    out_proj_grad = lax.psum_scatter(
        lax.dot_general(stream, retained, along, preferred_element_type=f32).astype(jnp.bfloat16),
        "sp",
        scatter_dimension=0,
        tiled=True,
    ).astype(jnp.float32)
    heads_here = log_decay.shape[1]
    key_dim = queries.shape[1] // heads_here
    value_dim = values.shape[1] // heads_here
    query_rows = queries.astype(f32).reshape(tokens_here, heads_here, key_dim)
    key_matrix = keys.astype(f32).reshape(tokens_here, heads_here, key_dim)
    value_matrix = values.astype(f32).reshape(tokens_here, heads_here, value_dim)
    incoming_gradient = ret_grad.astype(f32).reshape(tokens_here, heads_here, value_dim)
    running_total = jnp.cumsum(log_decay, axis=0)
    last_sum = running_total[-1]
    place = jnp.arange(tokens_here)
    causal = (place[:, None] >= place[None, :])[:, :, None]
    diff = running_total[:, None, :] - running_total[None, :, :]
    decay = jnp.where(causal, jnp.exp(jnp.minimum(diff, 0.0)), 0.0)
    scores = jnp.einsum("thk,shk->tsh", query_rows, key_matrix, precision=upper_limit) * decay
    prob_grad = (
        jnp.einsum("thv,shv->tsh", incoming_gradient, value_matrix, precision=upper_limit) * decay
    )
    added_input = jnp.einsum(
        "yb,ybm,ybx->bmx",
        jnp.exp(running_total),
        query_rows,
        incoming_gradient,
        precision=upper_limit,
    )
    block_multiplier = jnp.exp(last_sum)
    _, state_gradient = carried_in(
        (block_multiplier, added_input),
        "sp",
        combine_states,
        (jnp.ones_like(block_multiplier), jnp.zeros_like(added_input)),
    )
    tail = jnp.exp(last_sum[None, :] - running_total)[..., None]
    query_grad = jnp.einsum("tsh,shk->thk", prob_grad, key_matrix, precision=upper_limit) + jnp.exp(
        running_total
    )[..., None] * jnp.einsum(
        "ybc,bfc->ybf", incoming_gradient, incoming_state[0], precision=upper_limit
    )
    key_grad = jnp.einsum(
        "tsh,thk->shk", prob_grad, query_rows, precision=upper_limit
    ) + tail * jnp.einsum("rgd,gnd->rgn", value_matrix, state_gradient, precision=upper_limit)
    value_grad = jnp.einsum(
        "tsh,thv->shv", scores, incoming_gradient, precision=upper_limit
    ) + tail * jnp.einsum("bgi,gie->bge", key_matrix, state_gradient, precision=upper_limit)
    return (
        gate_w_grad[None],
        up_w_grad[None],
        down_grad[None],
        out_proj_grad,
        query_grad.reshape(tokens_here, -1).astype(bf16),
        key_grad.reshape(tokens_here, -1).astype(bf16),
        value_grad.reshape(tokens_here, -1).astype(bf16),
    )


def solution(mesh):
    placed = (
        P("sp", None),
        P("sp", "tp"),
        P("sp", None),
        P("sp", None),
        P("sp", None, "tp"),
        P("sp", None, "tp"),
        P("sp", "tp", None),
        P("tp", None),
        P("sp", "tp"),
        P("sp", "tp"),
        P("sp", "tp"),
        P("sp", "tp"),
        P("sp", "tp"),
        P("sp", "tp", None, None),
    )
    return jax.shard_map(
        on_device,
        mesh=mesh,
        in_specs=placed,
        out_specs=(
            P("sp", None, "tp"),
            P("sp", None, "tp"),
            P("sp", "tp", None),
            P("sp", "tp"),
            P("sp", "tp"),
            P("sp", "tp"),
            P("sp", "tp"),
        ),
        check_vma=False,
    )
```

profile of v0, /device:TPU:0, one launch (start us, length us, event | category | flops | bytes accessed | tf_op | source)
XLA Modules:
  0.0 227.4 jit_solution(18031763401095627964)
XLA Ops:
  10.8 1.3 convolution_convert_fusion.4
  12.2 21.6 %all_to_all.36 = bf16[8,60,512]{2,1,0:T(8,128)(2,1)S(1)} all-to-all(bf16[8,60,512]{2,1,0:T(8,128)(2,1)S(1)} %all_to_all.24), channel_id=1, replica_groups=mesh['sp'=8,'tp'=4] {'sp'}, dimensions={0} | all-to-all | bytes 983040 | tf_op jit(solution)/shard_map/all_to_all | solution.py:92
  35.7 17.5 %all_to_all.37 = bf16[8,60,512]{2,1,0:T(8,128)(2,1)S(1)} all-to-all(bf16[8,60,512]{2,1,0:T(8,128)(2,1)S(1)} %all_to_all.27), channel_id=1, replica_groups=mesh['sp'=8,'tp'=4] {'sp'}, dimensions={0} | all-to-all | bytes 983040 | tf_op jit(solution)/shard_map/all_to_all | solution.py:93
  54.2 1.6 all-gather.5.cloned.1.call-done
  55.8 3.8 %fusion.6 = f32[480,512]{1,0:T(8,128)} fusion(bf16[480,2048]{1,0:T(8,128)(2,1)} %all-gather.5.cloned.1.call-done, bf16[1,2048,512]{2,1,0:T(8,128)(2,1)S(1)} %copy-done), kind=kOutput, calls=%fused_computation.13 | convolution fusion | flops 1006632960 | bytes 5046272 | tf_op jit(solution)/shard_map/dot_general | solution.py:26
  59.6 2.2 fusion.9
  61.7 18.0 %all-gather.7.cloned.1.call-done = bf16[480,2048]{1,0:T(8,128)(2,1)} async-done(((bf16[480,512]{1,0:T(8,128)(2,1)}), bf16[480,2048]{1,0:T(8,128)(2,1)}) %all-gather.7.cloned.1.call-update) | async-done | bytes 1966096 | tf_op jit(solution)/shard_map/all_gather | solution.py:97
  79.7 4.2 %multiply_convert_fusion.1 = (bf16[480,512]{1,0:T(8,128)(2,1)S(1)}, bf16[480,512]{1,0:T(8,128)(2,1)S(1)}) fusion(f32[480,512]{1,0:T(8,128)} %fusion.6, f32[480,512]{1,0:T(8,128)} %fusion.9, bf16[480,2048]{1,0:T(8,128)(2,1)} %all-gather.7.cloned.1.call-done, bf16[1,512,2048]{2,1,0:T(8,128)(2,1)} %param.22), kind=kOutput, calls=%fused_computation.46 | convolution fusion | flops 1009827840 | bytes 7012352 | tf_op jit(solution)/shard_map/dot_general | solution.py:33
  84.0 1.2 fusion.4
  85.7 2.5 %add_convert_fusion = bf16[480,2048]{1,0:T(8,128)(2,1)} fusion(f32[480,2048]{1,0:T(8,128)S(1)} %fusion.4, bf16[480,512]{1,0:T(8,128)(2,1)S(1)} %get-tuple-element.242, bf16[1,2048,512]{2,1,0:T(8,128)(2,1)S(1)} %copy-done.2), kind=kOutput, calls=%fused_computation.3 | convolution fusion | flops 1008599040 | bytes 8486912 | tf_op jit(solution)/shard_map/dot_general | solution.py:41
  88.3 1.2 reduce-window.16
  91.2 20.5 %all-gather.1 = f32[8,1,4]{2,1,0:T(1,128)S(1)} all-gather(f32[1,1,4]{2,1,0:T(1,128)S(1)} %bitcast.153), channel_id=1, replica_groups=mesh['sp'=8,'tp'=4] {'sp'}, dimensions={0}, use_global_device_ids=true | all-gather | bytes 144 | tf_op jit(solution)/shard_map/all_gather | solution.py:9
  112.3 1.3 fusion.13
  113.6 5.2 %reduce-scatter.3.cloned.1.call-done = bf16[480,512]{1,0:T(8,128)(2,1)} async-done(((bf16[480,2048]{1,0:T(8,128)(2,1)}), bf16[480,512]{1,0:T(8,128)(2,1)}) %reduce-scatter.3.cloned.1.call-update) | async-done | bytes 491536 | tf_op jit(solution)/shard_map/reduce_scatter | solution.py:103
  118.8 1.9 all_to_all.30
  120.7 5.5 %all-to-all-start.2 = ((bf16[8,60,512]{2,1,0:T(8,128)(2,1)}), bf16[8,60,512]{2,1,0:T(8,128)(2,1)S(1)}, u32[]{:S(2)}, u32[]{:S(2)}) async-start(bf16[8,60,512]{2,1,0:T(8,128)(2,1)} %all_to_all.30), calls=%async_computation.3 | async-start | bytes 1048576 | tf_op jit(solution)/shard_map/all_to_all | solution.py:107
  126.5 4.3 %fusion.1 = bf16[1,2048,512]{2,1,0:T(8,128)(2,1)} fusion(bf16[480,2048]{1,0:T(8,128)(2,1)} %all-gather.5.cloned.1.call-done, bf16[480,512]{1,0:T(8,128)(2,1)S(1)} %get-tuple-element.243), kind=kOutput, calls=%fused_computation.8 | convolution fusion | flops 1007681536 | bytes 4554752 | tf_op jit(solution)/shard_map/dot_general | solution.py:37
  130.8 2.6 %fusion.2 = bf16[1,2048,512]{2,1,0:T(8,128)(2,1)} fusion(bf16[480,2048]{1,0:T(8,128)(2,1)S(1)} %copy-done.14, bf16[480,512]{1,0:T(8,128)(2,1)S(1)} %copy-done.4), kind=kOutput, calls=%fused_computation.9 | convolution fusion | flops 1007681536 | bytes 4554752 | tf_op jit(solution)/shard_map/dot_general | solution.py:38
  133.4 2.7 %fusion.3 = bf16[1,512,2048]{2,1,0:T(8,128)(2,1)} fusion(bf16[480,2048]{1,0:T(8,128)(2,1)S(1)} %copy-done.15, f32[480,512]{1,0:T(8,128)S(1)} %copy-done.17, f32[480,512]{1,0:T(8,128)S(1)} %copy-done.16), kind=kOutput, calls=%fused_computation.10 | convolution fusion | flops 1009156096 | bytes 6029312 | tf_op jit(solution)/shard_map/dot_general | solution.py:36
  136.1 4.4 %all-to-all-done.2 = bf16[8,60,512]{2,1,0:T(8,128)(2,1)S(1)} async-done(((bf16[8,60,512]{2,1,0:T(8,128)(2,1)}), bf16[8,60,512]{2,1,0:T(8,128)(2,1)S(1)}, u32[]{:S(2)}, u32[]{:S(2)}) %all-to-all-start.2) | async-done | bytes 491552 | tf_op jit(solution)/shard_map/all_to_all | solution.py:107
  140.6 1.2 fusion.18
  141.8 7.7 %all_gather.21 = bf16[192,2048]{1,0:T(8,128)(2,1)S(1)} all-gather(bf16[192,512]{1,0:T(8,128)(2,1)S(1)} %fusion.18), channel_id=1, replica_groups=mesh['sp'=8,'tp'=4] {'tp'}, dimensions={1}, use_global_device_ids=true | all-gather | bytes 983040 | tf_op jit(solution)/shard_map/all_gather | solution.py:110
  149.5 2.8 %convolution_convert_fusion.3 = bf16[2048,384]{1,0:T(8,128)(2,1)} fusion(bf16[192,2048]{1,0:T(8,128)(2,1)S(1)} %all_gather.21, bf16[192,384]{1,0:T(8,128)(2,1)} %param.24), kind=kOutput, calls=%fused_computation.7 | convolution fusion | flops 302776320 | bytes 2506752 | tf_op jit(solution)/shard_map/dot_general | solution.py:115
  152.3 2.1 convolution_convert_fusion.5
  155.1 1.3 fusion.14
  157.6 1.6 copy.162
  159.3 35.0 %all-gather = f32[32,48,96]{2,1,0:T(8,128)} all-gather(f32[4,48,96]{2,1,0:T(8,128)S(1)} %fusion.28), channel_id=2, replica_groups=mesh['sp'=8,'tp'=4] {'sp'}, dimensions={0}, use_global_device_ids=true | all-gather | bytes 663552 | tf_op jit(solution)/shard_map/all_gather | solution.py:9
  194.3 8.2 %while.16 = (s32[]{:T(128)}, f32[4,48,96]{2,1,0:T(8,128)S(1)}, s32[]{:T(128)}, f32[8,4,48,96]{3,2,1,0:T(8,128)}, f32[8,4]{1,0:T(8,128)S(1)}, /*index=5*/s32[]{:T(128)}, s32[]{:T(128)}, s32[]{:T(128)}, s32[]{:T(128)}) while((s32[]{:T(128)}, f32[4,48,96]{2,1,0:T(8,128)S(1)}, s32[]{:T(128)}, f32[8,4,48,96]{3,2,1,0:T(8,128)}, ...), condition=%wide.region_10.11_spmd.clone, body=%wide.region_9.10_spmd.clone.sunk | while | flops 73736 | bytes 221407 | solution.py:20
  202.5 1.4 fusion.22
  205.1 1.6 convolution_bitcast_fusion.3
  207.8 11.4 %reduce-scatter.5.cloned.1.call-done = bf16[256,384]{1,0:T(8,128)(2,1)} async-done(((bf16[2048,384]{1,0:T(8,128)(2,1)}), bf16[256,384]{1,0:T(8,128)(2,1)}) %reduce-scatter.5.cloned.1.call-update) | async-done | bytes 196624 | tf_op jit(solution)/shard_map/reduce_scatter | solution.py:114
  219.2 1.7 convert_element_type.88
  (106 shorter events, 21.7 us)
Async XLA Ops:
  7.2 48.6 %copy-start = (bf16[1,2048,512]{2,1,0:T(8,128)(2,1)S(1)}, bf16[1,2048,512]{2,1,0:T(8,128)(2,1)}, u32[]{:S(2)}) copy-start(bf16[1,2048,512]{2,1,0:T(8,128)(2,1)} %param.20) | copy-start | bytes 6291460
  7.2 48.6 %all-gather.5.cloned.1.call-start = ((), (), s32[]{:S(2)}) async-start(), calls=%async_computation.5 | async-start | bytes 2457600 | tf_op jit(solution)/shard_map/all_gather | solution.py:96
  10.8 24.0 %copy-start.12 = (f32[192,2]{0,1:T(2,128)S(1)}, f32[192,2]{0,1:T(2,128)}, u32[]{:S(2)}) copy-start(f32[192,2]{0,1:T(2,128)} %param.19) | copy-start | bytes 4612
  10.8 24.4 %copy-start.5 = (bf16[192,512]{1,0:T(8,128)(2,1)S(1)}, bf16[192,512]{1,0:T(8,128)(2,1)}, u32[]{:S(2)}) copy-start(bf16[192,512]{1,0:T(8,128)(2,1)} %param.17) | copy-start | bytes 589828
  34.7 45.0 %all-gather.7.cloned.1.call-start = ((), (), s32[]{:S(2)}) async-start(), calls=%async_computation.6 | async-start | bytes 2457600 | tf_op jit(solution)/shard_map/all_gather | solution.py:97
  54.1 64.7 %reduce-scatter.3.cloned.1.call-start = ((), (), s32[]{:S(2)}) async-start(), calls=%async_computation.7 | async-start | bytes 2457600 | tf_op jit(solution)/shard_map/reduce_scatter | solution.py:103
  55.7 3.8 %copy-start.1 = (bf16[1,2048,512]{2,1,0:T(8,128)(2,1)S(1)}, bf16[1,2048,512]{2,1,0:T(8,128)(2,1)}, u32[]{:S(2)}) copy-start(bf16[1,2048,512]{2,1,0:T(8,128)(2,1)} %param.21) | copy-start | bytes 6291460
  55.7 3.8 %copy-start.13 = (bf16[480,2048]{1,0:T(8,128)(2,1)S(1)}, bf16[480,2048]{1,0:T(8,128)(2,1)}, u32[]{:S(2)}) copy-start(bf16[480,2048]{1,0:T(8,128)(2,1)} %all-gather.5.cloned.1.call-done) | copy-start | bytes 5898244
  83.9 1.2 copy-start.3
  83.9 1.8 copy-start.2
  85.7 2.5 %copy-start.11 = (f32[192,4]{0,1:T(4,128)S(1)}, f32[192,4]{0,1:T(4,128)}, u32[]{:S(2)}) copy-start(f32[192,4]{0,1:T(4,128)} %param.28) | copy-start | bytes 9220
  88.2 1.7 copy-start.6
  88.2 2.5 %copy-start.7 = (bf16[192,192]{1,0:T(8,128)(2,1)S(1)}, bf16[192,192]{1,0:T(8,128)(2,1)}, u32[]{:S(2)}) copy-start(bf16[192,192]{1,0:T(8,128)(2,1)} %param.26) | copy-start | bytes 221188
  88.2 2.6 %copy-start.8 = (bf16[192,192]{1,0:T(8,128)(2,1)S(1)}, bf16[192,192]{1,0:T(8,128)(2,1)}, u32[]{:S(2)}) copy-start(bf16[192,192]{1,0:T(8,128)(2,1)} %param.25) | copy-start | bytes 221188
  111.7 0.6 copy-start.10
  120.7 19.8 %all-to-all-start.2 = ((bf16[8,60,512]{2,1,0:T(8,128)(2,1)}), bf16[8,60,512]{2,1,0:T(8,128)(2,1)S(1)}, u32[]{:S(2)}, u32[]{:S(2)}) async-start(bf16[8,60,512]{2,1,0:T(8,128)(2,1)} %all_to_all.30), calls=%async_computation.3 | async-start | bytes 1048576 | tf_op jit(solution)/shard_map/all_to_all | solution.py:107
  126.2 93.0 %reduce-scatter.5.cloned.1.call-start = ((), (), s32[]{:S(2)}) async-start(), calls=%async_computation.8 | async-start | bytes 1769472 | tf_op jit(solution)/shard_map/reduce_scatter | solution.py:114
  126.4 4.3 %copy-start.4 = (bf16[480,512]{1,0:T(8,128)(2,1)S(1)}, bf16[480,512]{1,0:T(8,128)(2,1)}, u32[]{:S(2)}) copy-start(bf16[480,512]{1,0:T(8,128)(2,1)} %copy-done.3) | copy-start | bytes 1474564
  126.5 4.3 %copy-start.14 = (bf16[480,2048]{1,0:T(8,128)(2,1)S(1)}, bf16[480,2048]{1,0:T(8,128)(2,1)}, u32[]{:S(2)}) copy-start(bf16[480,2048]{1,0:T(8,128)(2,1)} %all-gather.5.cloned.1.call-done) | copy-start | bytes 5898244
  130.8 2.7 %copy-start.15 = (bf16[480,2048]{1,0:T(8,128)(2,1)S(1)}, bf16[480,2048]{1,0:T(8,128)(2,1)}, u32[]{:S(2)}) copy-start(bf16[480,2048]{1,0:T(8,128)(2,1)} %all-gather.7.cloned.1.call-done) | copy-start | bytes 5898244
  130.8 2.7 %copy-start.16 = (f32[480,512]{1,0:T(8,128)S(1)}, f32[480,512]{1,0:T(8,128)}, u32[]{:S(2)}) copy-start(f32[480,512]{1,0:T(8,128)} %fusion.6) | copy-start | bytes 2949124
  130.8 2.7 %copy-start.17 = (f32[480,512]{1,0:T(8,128)S(1)}, f32[480,512]{1,0:T(8,128)}, u32[]{:S(2)}) copy-start(f32[480,512]{1,0:T(8,128)} %fusion.9) | copy-start | bytes 2949124
  152.3 2.6 %copy-start.9 = (f32[1,4,48,96]{3,2,1,0:T(8,128)S(1)}, f32[1,4,48,96]{3,2,1,0:T(8,128)}, u32[]{:S(2)}) copy-start(f32[1,4,48,96]{3,2,1,0:T(8,128)} %param.29) | copy-start | bytes 221188
Sparse Core Ops, SparseCore 0:
  34.8 20.8 all-gather.4
  57.9 21.8 all-gather.6
  88.4 30.3 reduce-scatter.2
  152.4 66.6 reduce-scatter.4
where the time goes:
time: 228 us; the launch traced here: 227 us
  blocking collectives  102 us (45%)
  waiting for transfers between devices  40.6 us (18%)
  matrix products  39.3 us (17%)
  between operations  14.1 us (6%)
  other arithmetic  13 us (6%)
  local copies, waits for them, and re-layouts  11.9 us (5%)
  starting transfers between devices  5.85 us (3%)
    all_gather x2, blocking collectives, carried_in(): everything = jax.tree.map(lambda part: lax.all_gather(part, axis), x)  55.5 us
    all_to_all x1, blocking collectives, on_device(): lax.all_to_all(send_rows, 'sp', split_axis=0, concat_axis=0, tiled=True)  21.6 us
    all_gather x1, waiting for transfers between devices, on_device(): lax.all_gather(part_grad, 'tp', axis=1, tiled=True)  18 us
    all_to_all x1, blocking collectives, on_device(): lax.all_to_all(send_grad, 'sp', split_axis=0, concat_axis=0, tiled=True)  17.5 us
    reduce_scatter x1, waiting for transfers between devices, on_device(): lax.psum_scatter(lax.dot_general(stream, retained, along, preferred_eleme...  11.4 us
    select_n x8, other arithmetic, lap(): return jax.tree.map(lambda a, b: jnp.where(reached, a, b), new, before)  7.84 us
    all_gather x1, blocking collectives, on_device(): stream = lax.all_gather(stream_part, 'tp', axis=1, tiled=True)  7.66 us
    unnamed x44, local copies, waits for them, and re-layouts  5.57 us
  transfers between devices with their start and end apart: 5, of which 5 were waited for; matrix products, arithmetic and copies ran while one was open for 18% of the time, Pallas kernels for 0%

commit v1 on v0

--- a/solution.py
+++ b/solution.py
@@ -1,23 +1,333 @@
+import functools
+
 import jax
 import jax.numpy as jnp
 from jax import lax
+from jax.experimental import pallas as pl
+from jax.experimental.pallas import tpu as pltpu
 from jax.sharding import PartitionSpec as P
 
-
-def carried_in(x, axis, combine, identity):
-    devices, place = (lax.axis_size(axis), lax.axis_index(axis))
-    everything = jax.tree.map(lambda part: lax.all_gather(part, axis), x)
-    start = jax.tree.map(
-        lambda part, zero: jnp.broadcast_to(jnp.asarray(zero, part.dtype), part.shape), x, identity
-    )
-
-    def lap(k, before):
-        at = devices - 1 - k
-        reached = at > place
-        new = combine(before, jax.tree.map(lambda part: part[at], everything))
-        return jax.tree.map(lambda a, b: jnp.where(reached, a, b), new, before)
-
-    return lax.fori_loop(0, devices, lap, start)
+MESH = pl.DeviceIdType.MESH
+F32 = jnp.float32
+BF16 = jnp.bfloat16
+LIMIT = 60 * 1024 * 1024
+
+
+def where_am_i(n, ny):
+    s, t = lax.axis_index("sp"), lax.axis_index("tp")
+    return s, t, lax.div(t, 2), lax.rem(t, 2)
+
+
+def greet(peers):
+    barrier = pltpu.get_barrier_semaphore()
+    for peer in peers:
+        pl.semaphore_signal(barrier, inc=1, device_id=peer, device_id_type=MESH)
+    pl.semaphore_wait(barrier, len(peers))
+
+
+def sp_peers(n, s, t):
+    return [(lax.rem(s + k, n), t) for k in range(1, n)]
+
+
+def tp_peers(ny, s, y, c):
+    return [(s, lax.rem(y + d, ny) * 2 + c) for d in range(1, ny)] + [(s, y * 2 + 1 - c)]
+
+
+def remote(src, dst, send, recv, peer):
+    return pltpu.make_async_remote_copy(
+        src_ref=src, dst_ref=dst, send_sem=send, recv_sem=recv, device_id=peer, device_id_type=MESH
+    )
+
+
+def dispatch_kernel(
+    n, ny, send_ref, kept_ref, ends_ref, out_ref, kept_out, ends_out,
+    local_sem, a_send, a_recv, e_send, e_recv, y_send, y_recv, p_send, p_recv,
+    r_send, r_recv, l_send, l_recv, x_send, x_recv,
+):
+    s, t, y, c = where_am_i(n, ny)
+    cap, q = send_ref.shape[2], send_ref.shape[3]
+    nz = n // 2
+    z, x = lax.div(s, 2), lax.rem(s, 2)
+    greet(sp_peers(n, s, t) + tp_peers(ny, s, y, c))
+    partner = (s, y * 2 + 1 - c)
+
+    def block(src, tt):
+        rows = pl.ds(pl.multiple_of(src * cap, cap), cap)
+        columns = pl.ds(pl.multiple_of(tt * q, q), q)
+        return out_ref.at[:, rows, columns]
+
+    own = [
+        pltpu.make_async_copy(send_ref.at[s], block(s, t), local_sem.at[0]),
+        pltpu.make_async_copy(kept_ref, kept_out.at[s], local_sem.at[1]),
+        pltpu.make_async_copy(ends_ref, ends_out.at[s], local_sem.at[2]),
+    ]
+    for copy in own:
+        copy.start()
+    arrivals, waits = [own[0]], []
+    for k in range(1, n):
+        peer = lax.rem(s + k, n)
+        copy = remote(send_ref.at[peer], block(s, t), a_send.at[k], a_recv.at[k], (peer, t))
+        copy.start()
+        arrivals.append(copy)
+        waits.append(copy.wait_send)
+    for k in range(1, n):
+        peer = lax.rem(s + k, n)
+        copy = remote(ends_ref, ends_out.at[s], e_send.at[k], e_recv.at[k], (peer, t))
+        copy.start()
+        waits.append(copy.wait)
+
+    def at(zz):
+        return lax.rem(zz + 2 * nz, nz) * 2 + x
+
+    def hop(j, sign, send, recv, source):
+        held = at(z - sign * j)
+        copy = remote(source, kept_out.at[held], send.at[j], recv.at[j], (at(z + sign), t))
+        copy.start()
+        waits.append(copy.wait_send)
+        return copy
+
+    right_steps, left_steps = nz // 2, nz - 1 - nz // 2
+    right = hop(0, 1, r_send, r_recv, kept_ref) if right_steps else None
+    left = hop(0, -1, l_send, l_recv, kept_ref) if left_steps else None
+    pair = (z * 2 + 1 - x, t)
+
+    def across(held, index, source):
+        copy = remote(source, kept_out.at[held], x_send.at[index], x_recv.at[index], pair)
+        copy.start()
+        waits.append(copy.wait)
+
+    across(s, 0, kept_ref)
+    from_far = {}
+    for k in range(n + 1):
+        if k < n:
+            src = lax.rem(s - k + n, n)
+            if k == 0:
+                arrivals[0].wait()
+            else:
+                arrivals[k].wait_recv()
+            mine = block(src, t)
+            for d in range(1, ny):
+                far = (s, lax.rem(y + d, ny) * 2 + c)
+                copy = remote(mine, mine, y_send.at[d, k], y_recv.at[d, k], far)
+                copy.start()
+                waits.append(copy.wait_send)
+                from_far[d, k] = copy
+            copy = remote(mine, mine, p_send.at[0, k], p_recv.at[0, k], partner)
+            copy.start()
+            waits.append(copy.wait)
+        if k >= 1:
+            src = lax.rem(s - k + 1 + n, n)
+            for d in range(1, ny):
+                from_far[d, k - 1].wait_recv()
+                theirs = block(src, lax.rem(y - d + ny, ny) * 2 + c)
+                copy = remote(theirs, theirs, p_send.at[d, k - 1], p_recv.at[d, k - 1], partner)
+                copy.start()
+                waits.append(copy.wait)
+    index = 1
+    for j in range(1, right_steps + 1):
+        right.wait_recv()
+        held = at(z - j)
+        if j < right_steps:
+            right = hop(j, 1, r_send, r_recv, kept_out.at[held])
+        across(held, index, kept_out.at[held])
+        index += 1
+        if j <= left_steps:
+            left.wait_recv()
+            held = at(z + j)
+            if j < left_steps:
+                left = hop(j, -1, l_send, l_recv, kept_out.at[held])
+            across(held, index, kept_out.at[held])
+            index += 1
+    own[1].wait()
+    own[2].wait()
+    for wait in waits:
+        wait()
+
+
+def dispatch(n, ny, send, kept, ends):
+    cap, q = send.shape[2], send.shape[3]
+    dma = pltpu.SemaphoreType.DMA
+    return pl.pallas_call(
+        functools.partial(dispatch_kernel, n, ny),
+        out_shape=(
+            jax.ShapeDtypeStruct((2, n * cap, q * ny * 2), BF16),
+            jax.ShapeDtypeStruct((n,) + kept.shape, BF16),
+            jax.ShapeDtypeStruct((n,) + ends.shape, F32),
+        ),
+        in_specs=[pl.BlockSpec(memory_space=pltpu.VMEM)] * 3,
+        out_specs=[pl.BlockSpec(memory_space=pltpu.VMEM)] * 3,
+        scratch_shapes=[dma((3,)), dma((n,)), dma((n,)), dma((n,)), dma((n,))]
+        + [dma((ny, n))] * 4
+        + [dma((n,))] * 6,
+        compiler_params=pltpu.CompilerParams(
+            collective_id=0, has_side_effects=True, vmem_limit_bytes=LIMIT
+        ),
+    )(send, kept, ends)
+
+
+def combine_kernel(
+    n, ny, part_ref, pick_ref, grad_ref, stream_ref, near, pairs, far, share, back,
+    p_send, p_recv, y_send, y_recv, a_send, a_recv, g_send, g_recv, h_send, h_recv,
+):
+    s, t, y, c = where_am_i(n, ny)
+    q = grad_ref.shape[1]
+    cap = part_ref.shape[0] // n
+    greet(sp_peers(n, s, t) + tp_peers(ny, s, y, c))
+    partner = (s, y * 2 + 1 - c)
+    waits = []
+
+    def columns(tt):
+        return pl.ds(pl.multiple_of(tt * q, q), q)
+
+    def rows(b):
+        return pl.ds(pl.multiple_of(b * cap, cap), cap)
+
+    halves = {}
+    for d in list(range(1, ny)) + [0]:
+        theirs = lax.rem(y + d, ny) * 2 + 1 - c
+        copy = remote(
+            part_ref.at[:, columns(theirs)], near.at[d], p_send.at[d], p_recv.at[d], partner
+        )
+        copy.start()
+        waits.append(copy.wait_send)
+        halves[d] = copy
+    arrived = {}
+    for d in range(1, ny):
+        halves[d].wait_recv()
+        tt = lax.rem(y + d, ny) * 2 + c
+        for k in range(1, n + 1):
+            b = rows(lax.rem(s + k, n))
+            pairs[d, b, :] = (
+                part_ref[b, columns(tt)].astype(F32) + near[d, b, :].astype(F32)
+            ).astype(BF16)
+        for k in range(1, n + 1):
+            b = rows(lax.rem(s + k, n))
+            copy = remote(
+                pairs.at[d, b, :], far.at[d, b, :],
+                y_send.at[d, k % n], y_recv.at[d, k % n], (s, tt),
+            )
+            copy.start()
+            waits.append(copy.wait_send)
+            arrived[d, k] = copy
+    halves[0].wait_recv()
+    returns = []
+    for k in range(1, n + 1):
+        peer = lax.rem(s + k, n)
+        b = rows(peer)
+        total = part_ref[b, columns(t)].astype(F32) + near[0, b, :].astype(F32)
+        for d in range(1, ny):
+            arrived[d, k].wait_recv()
+            total = total + far[d, b, :].astype(F32)
+        if k < n:
+            share[b, :] = total.astype(BF16)
+            copy = remote(
+                share.at[b, :], back.at[rows(s), :], a_send.at[k], a_recv.at[k], (peer, t)
+            )
+            copy.start()
+            waits.append(copy.wait_send)
+            returns.append(copy)
+        else:
+            back[b, :] = total.astype(BF16)
+    for copy in returns:
+        copy.wait_recv()
+    token = jnp.dot(pick_ref[...], back[...], preferred_element_type=F32)
+    stream_ref[:, columns(t)] = (grad_ref[...].astype(F32) + token).astype(BF16)
+    mine = stream_ref.at[:, columns(t)]
+    outer = []
+    for d in range(1, ny):
+        copy = remote(
+            mine, mine, g_send.at[d], g_recv.at[d], (s, lax.rem(y + d, ny) * 2 + c)
+        )
+        copy.start()
+        waits.append(copy.wait_send)
+        outer.append(copy)
+    copy = remote(mine, mine, h_send.at[0], h_recv.at[0], partner)
+    copy.start()
+    waits.append(copy.wait)
+    for d in range(1, ny):
+        outer[d - 1].wait_recv()
+        theirs = stream_ref.at[:, columns(lax.rem(y - d + ny, ny) * 2 + c)]
+        copy = remote(theirs, theirs, h_send.at[d], h_recv.at[d], partner)
+        copy.start()
+        waits.append(copy.wait)
+    for wait in waits:
+        wait()
+
+
+def combine(n, ny, part, pick, grad):
+    slots, q = part.shape[0], grad.shape[1]
+    dma = pltpu.SemaphoreType.DMA
+    return pl.pallas_call(
+        functools.partial(combine_kernel, n, ny),
+        out_shape=jax.ShapeDtypeStruct((grad.shape[0], q * ny * 2), BF16),
+        in_specs=[pl.BlockSpec(memory_space=pltpu.VMEM)] * 3,
+        out_specs=pl.BlockSpec(memory_space=pltpu.VMEM),
+        scratch_shapes=[pltpu.VMEM((ny, slots, q), BF16)] * 3
+        + [pltpu.VMEM((slots, q), BF16)] * 2
+        + [dma((ny,))] * 2
+        + [dma((ny, n))] * 2
+        + [dma((n,))] * 2
+        + [dma((ny,))] * 4,
+        compiler_params=pltpu.CompilerParams(
+            collective_id=1, has_side_effects=True, vmem_limit_bytes=LIMIT
+        ),
+    )(part, pick, grad)
+
+
+def tail_kernel(
+    n, ny, stream_ref, state_ref, cols_ref, states_ref,
+    local_sem, a_send, a_recv, i_send, i_recv, p_send, p_recv,
+):
+    s, t, y, c = where_am_i(n, ny)
+    half = stream_ref.shape[1] // 2
+    partner = (s, y * 2 + 1 - c)
+    greet(sp_peers(n, s, t) + [partner])
+    band = pl.ds(pl.multiple_of(c * half, half), half)
+    own = [
+        pltpu.make_async_copy(stream_ref.at[s], cols_ref.at[s], local_sem.at[0]),
+        pltpu.make_async_copy(state_ref, states_ref.at[s], local_sem.at[1]),
+    ]
+    for copy in own:
+        copy.start()
+    waits, arrivals = [copy.wait for copy in own], []
+    for k in range(1, n):
+        peer = lax.rem(s + k, n)
+        copy = remote(state_ref, states_ref.at[s], i_send.at[k], i_recv.at[k], (peer, t))
+        copy.start()
+        waits.append(copy.wait)
+    for k in range(1, n):
+        peer = lax.rem(s + k, n)
+        copy = remote(
+            stream_ref.at[peer, band], cols_ref.at[s, band], a_send.at[k], a_recv.at[k], (peer, t)
+        )
+        copy.start()
+        waits.append(copy.wait_send)
+        arrivals.append(copy)
+    for k in range(1, n):
+        arrivals[k - 1].wait_recv()
+        held = cols_ref.at[lax.rem(s - k + n, n), band]
+        copy = remote(held, held, p_send.at[k], p_recv.at[k], partner)
+        copy.start()
+        waits.append(copy.wait)
+    for wait in waits:
+        wait()
+
+
+def tail_exchange(n, ny, stream, state):
+    dma = pltpu.SemaphoreType.DMA
+    return pl.pallas_call(
+        functools.partial(tail_kernel, n, ny),
+        out_shape=(
+            jax.ShapeDtypeStruct(stream.shape, BF16),
+            jax.ShapeDtypeStruct((n,) + state.shape, state.dtype),
+        ),
+        in_specs=[pl.BlockSpec(memory_space=pltpu.VMEM)] * 2,
+        out_specs=[pl.BlockSpec(memory_space=pltpu.VMEM)] * 2,
+        scratch_shapes=[dma((2,))] + [dma((n,))] * 6,
+        compiler_params=pltpu.CompilerParams(
+            collective_id=2, has_side_effects=True, vmem_limit_bytes=LIMIT
+        ),
+    )(stream, state)
 
 
 def expert_back(rows, grad, gate_w, up_w, down_w):
@@ -40,10 +350,6 @@
         gate_grad, gate_w, across, preferred_element_type=f32
     ) + lax.dot_general(up_grad, up_w, across, preferred_element_type=f32)
     return (gate_w_grad, up_w_grad, down_grad, partial_value)
-
-
-def combine_states(earlier, later):
-    return (later[0] * earlier[0], later[1] + later[0][:, None, None] * earlier[1])
 
 
 def on_device(
@@ -69,7 +375,7 @@
     width = moe_input.shape[1]
     sp_count = lax.axis_size("sp")
     tp_count = lax.axis_size("tp")
-    capacity = 5 * tokens_here // (2 * sp_count)
+    capacity = -(-(5 * tokens_here // (2 * sp_count)) // 16) * 16
     slot_count = sp_count * capacity
     flat_ids = expert_ids.reshape(-1)
     flat_weights = expert_weights.reshape(-1)
@@ -81,6 +387,10 @@
     slot_weight = jnp.sum(jnp.where(hits, flat_weights[None, :], 0.0), axis=1)
     along = (((0,), (0,)), ((), ()))
     column_count = width // tp_count
+    ny = tp_count // 2
+    heads_here = log_decay.shape[1]
+    running_total = jnp.cumsum(log_decay, axis=0)
+    last_sum = running_total[-1]
     own_rows = lax.dynamic_slice_in_dim(
         moe_input, lax.axis_index("tp") * column_count, column_count, 1
     )
@@ -88,44 +398,24 @@
     send_grad = (
         jnp.dot(picker, out_grad, preferred_element_type=f32) * slot_weight[:, None]
     ).astype(bf16)
-    part_rows, part_grad = (
-        lax.all_to_all(send_rows, "sp", split_axis=0, concat_axis=0, tiled=True),
-        lax.all_to_all(send_grad, "sp", split_axis=0, concat_axis=0, tiled=True),
-    )
-    recv_rows, recv_grad = (
-        lax.all_gather(part_rows, "tp", axis=1, tiled=True),
-        lax.all_gather(part_grad, "tp", axis=1, tiled=True),
-    )
+    send = jnp.stack(
+        [part.reshape(sp_count, capacity, column_count) for part in (send_rows, send_grad)], axis=1
+    )
+    ends = jnp.zeros((8, 128), f32).at[:, :heads_here].set(last_sum[None, :])
+    received, kept_all, ends_all = dispatch(sp_count, ny, send, retained, ends)
     gate_w_grad, up_w_grad, down_grad, partial_value = expert_back(
-        recv_rows, recv_grad, w_gate[0], w_up[0], w_down[0]
-    )
-    share = (
-        lax.psum_scatter(partial_value.astype(jnp.bfloat16), "tp", scatter_dimension=1, tiled=True)
-        .astype(jnp.float32)
-        .astype(bf16)
-    )
-    returned = lax.all_to_all(share, "sp", split_axis=0, concat_axis=0, tiled=True)
-    token_grad = lax.dot_general(picker, returned, along, preferred_element_type=f32)
-    stream_part = (out_grad.astype(f32) + token_grad).astype(bf16)
-    stream = lax.all_gather(stream_part, "tp", axis=1, tiled=True)
+        received[0], received[1], w_gate[0], w_up[0], w_down[0]
+    )
+    stream = combine(sp_count, ny, partial_value.astype(bf16), picker.T, out_grad)
     ret_grad = lax.dot_general(
         stream, out_proj, (((1,), (1,)), ((), ())), preferred_element_type=f32
     ).astype(bf16)
-    out_proj_grad = lax.psum_scatter(
-        lax.dot_general(stream, retained, along, preferred_element_type=f32).astype(jnp.bfloat16),
-        "sp",
-        scatter_dimension=0,
-        tiled=True,
-    ).astype(jnp.float32)
-    heads_here = log_decay.shape[1]
     key_dim = queries.shape[1] // heads_here
     value_dim = values.shape[1] // heads_here
     query_rows = queries.astype(f32).reshape(tokens_here, heads_here, key_dim)
     key_matrix = keys.astype(f32).reshape(tokens_here, heads_here, key_dim)
     value_matrix = values.astype(f32).reshape(tokens_here, heads_here, value_dim)
     incoming_gradient = ret_grad.astype(f32).reshape(tokens_here, heads_here, value_dim)
-    running_total = jnp.cumsum(log_decay, axis=0)
-    last_sum = running_total[-1]
     place = jnp.arange(tokens_here)
     causal = (place[:, None] >= place[None, :])[:, :, None]
     diff = running_total[:, None, :] - running_total[None, :, :]
@@ -141,13 +431,29 @@
         incoming_gradient,
         precision=upper_limit,
     )
-    block_multiplier = jnp.exp(last_sum)
-    _, state_gradient = carried_in(
-        (block_multiplier, added_input),
-        "sp",
-        combine_states,
-        (jnp.ones_like(block_multiplier), jnp.zeros_like(added_input)),
-    )
+    flat_state = added_input.transpose(1, 0, 2).reshape(key_dim, heads_here * value_dim)
+    stream_blocks = stream.reshape(tokens_here, sp_count, width // sp_count).transpose(1, 0, 2)
+    stream_all, states = tail_exchange(sp_count, ny, stream_blocks, flat_state.astype(bf16))
+    out_proj_grad = lax.dot_general(
+        stream_all.reshape(sp_count * tokens_here, -1),
+        kept_all.reshape(sp_count * tokens_here, -1),
+        along,
+        preferred_element_type=f32,
+    )
+    block_ends = ends_all[:, 0, :heads_here]
+    before = jnp.cumsum(block_ends, axis=0) - block_ends
+    here = lax.axis_index("sp")
+    since = jnp.sum(
+        jnp.where(jnp.arange(sp_count)[:, None] <= here, block_ends, 0.0), axis=0, keepdims=True
+    )
+    reach = jnp.where(
+        jnp.arange(sp_count)[:, None] > here, jnp.exp(jnp.minimum(before - since, 0.0)), 0.0
+    )
+    state_gradient = jnp.sum(
+        states.astype(f32).reshape(sp_count, key_dim, heads_here, value_dim)
+        * reach[:, None, :, None],
+        axis=0,
+    ).transpose(1, 0, 2)
     tail = jnp.exp(last_sum[None, :] - running_total)[..., None]
     query_grad = jnp.einsum("tsh,shk->thk", prob_grad, key_matrix, precision=upper_limit) + jnp.exp(
         running_total

time: 228 us -> 166 us (0.73)
  Pallas kernels: 0 us -> 112 us
  blocking collectives: 102 us -> 0 us
  waiting for transfers between devices: 40.6 us -> 0 us
  between operations: 14.1 us -> 1.06 us
  matrix products: 39.3 us -> 31.2 us
  starting transfers between devices: 5.85 us -> 0 us
  other arithmetic: 13 us -> 7.89 us
    pallas_call x0 -> x3, Pallas kernels: none -> 112 us  [the longest x1 59.9 us: dispatch(): pl.pallas_call(functools.partial(dispatch_kernel, n, ny), out_shape=(jax....]
    all_gather x3 -> x0, blocking collectives: 63.2 us -> none  [the longest x2 55.5 us: carried_in(): everything = jax.tree.map(lambda part: lax.all_gather(part, axis), x)]
    all_to_all x2 -> x0, blocking collectives: 39.1 us -> none  [the longest x1 21.6 us: on_device(): lax.all_to_all(send_rows, 'sp', split_axis=0, concat_axis=0, tiled=True)]
    all_gather x2 -> x0, waiting for transfers between devices: 19.6 us -> none  [the longest x1 18 us: on_device(): lax.all_gather(part_grad, 'tp', axis=1, tiled=True)]
    reduce_scatter x2 -> x0, waiting for transfers between devices: 16.6 us -> none  [the longest x1 11.4 us: on_device(): lax.psum_scatter(lax.dot_general(stream, retained, along, preferred_eleme...]
    select_n x8 -> x1, other arithmetic: 7.84 us -> 0.07 us  [on_device(): jnp.where(jnp.arange(sp_count)[:, None] > here, jnp.exp(jnp.minimum(befor...]
    all_to_all x1 -> x0, starting transfers between devices: 5.51 us -> none  [on_device(): lax.all_to_all(share, 'sp', split_axis=0, concat_axis=0, tiled=True)]
    all_to_all x1 -> x0, waiting for transfers between devices: 4.4 us -> none  [on_device(): lax.all_to_all(share, 'sp', split_axis=0, concat_axis=0, tiled=True)]
  transfers between devices with their start and end apart: 5 -> 0, of which waited for: 5 -> 0; matrix products, arithmetic and copies ran while one was open for 18% -> 0% of each run, Pallas kernels for 0% -> 0%
where the time goes in v1:
time: 166 us; the launch traced here: 164 us
  Pallas kernels  112 us (67%)
  matrix products  31.2 us (19%)
  local copies, waits for them, and re-layouts  11.7 us (7%)
  other arithmetic  7.89 us (5%)
    pallas_call x1, Pallas kernels, dispatch(): pl.pallas_call(functools.partial(dispatch_kernel, n, ny), out_shape=(jax....  59.9 us
    pallas_call x1, Pallas kernels, combine(): pl.pallas_call(functools.partial(combine_kernel, n, ny), out_shape=jax.Sh...  28.9 us
    pallas_call x1, Pallas kernels, tail_exchange(): pl.pallas_call(functools.partial(tail_kernel, n, ny), out_shape=(jax.Shap...  23.6 us
    unnamed x44, local copies, waits for them, and re-layouts  5.45 us
    dot_general x1, matrix products, expert_back(): lax.dot_general(act, grad, along, preferred_element_type=f32).astype(bf16)  4.48 us
    another operation x6, other arithmetic  3.45 us

profile of v1, /device:TPU:0, one launch (start us, length us, event | category | flops | bytes accessed | tf_op | source)
XLA Modules:
  0.0 164.2 jit_solution(681890137226683771)
XLA Ops:
  0.6 0.9 copy.131
  1.8 0.9 reduce-window.14
  3.1 0.8 copy.134
  4.5 0.7 multiply_add_fusion.1
  5.3 1.3 fusion.24
  6.6 1.3 convolution_convert_fusion.3
  7.9 1.1 pad_maximum_fusion.send_ref
  9.0 1.2 reduce-window.16
  11.4 0.6 broadcast_select_fusion
  12.7 59.9 %shard_map.189 = (bf16[2,512,2048]{2,1,0:T(8,128)(2,1)}, bf16[8,192,384]{2,1,0:T(8,128)(2,1)}, f32[8,8,128]{2,1,0:T(8,128)}) custom-call(bf16[8,2,64,512]{3,2,1,0:T(8,128)(2,1)} %pad_maximum_fusion.send_ref, bf16[192,384]{1,0:T(8,128)(2,1)} %kept_ref.1, f32[8,128]{1,0:T(8,128)} %scatter.8.ends_ref), custom_call_target="tpu_custom_call" | custom-call | tf_op jit(solution)/shard_map/pallas_call | solution.py:150
  72.6 3.0 %fusion.5 = f32[512,512]{1,0:T(8,128)S(1)} fusion(bf16[1,2048,512]{2,1,0:T(8,128)(2,1)S(1)} %copy-done, bf16[2,512,2048]{2,1,0:T(8,128)(2,1)} %get-tuple-element.24), kind=kOutput, calls=%fused_computation.9 | convolution fusion | flops 1073741824 | bytes 5242880 | tf_op jit(solution)/shard_map/dot_general | solution.py:336
  76.1 1.2 fusion.8
  77.3 0.7 copy-done.13
  78.0 1.6 multiply_convert_fusion.1
  79.7 1.3 fusion.3
  81.0 2.6 %add_convert_fusion.part_ref = bf16[512,2048]{1,0:T(8,128)(2,1)} fusion(f32[512,2048]{1,0:T(8,128)S(1)} %fusion.3, bf16[512,512]{1,0:T(8,128)(2,1)S(1)} %get-tuple-element.64, bf16[1,2048,512]{2,1,0:T(8,128)(2,1)S(1)} %copy-done.1), kind=kOutput, calls=%fused_computation | convolution fusion | flops 1075838976 | bytes 8912896 | tf_op jit(solution)/shard_map/dot_general | solution.py:351
  83.6 0.7 convert_bitcast_fusion.pick_ref
  84.3 28.9 %shard_map.190 = bf16[192,2048]{1,0:T(8,128)(2,1)} custom-call(bf16[512,2048]{1,0:T(8,128)(2,1)} %add_convert_fusion.part_ref, bf16[192,512]{1,0:T(8,128)(2,1)} %convert_bitcast_fusion.pick_ref, bf16[192,512]{1,0:T(8,128)(2,1)} %grad_ref.1), custom_call_target="tpu_custom_call" | custom-call | tf_op jit(solution)/shard_map/pallas_call | solution.py:260
  113.2 2.1 %copy.169 = bf16[24,8,8,256]{3,2,0,1:T(8,128)(2,1)} copy(bf16[24,8,8,256]{3,2,1,0:T(8,128)(2,1)} %bitcast.145) | data formatting | bytes 1572864 | tf_op jit(solution)/shard_map/reshape | solution.py:435
  115.3 1.8 %convolution_convert_fusion.4 = bf16[192,384]{1,0:T(8,128)(2,1)S(1)} fusion(bf16[192,2048]{1,0:T(8,128)(2,1)} %shard_map.190, bf16[384,2048]{1,0:T(8,128)(2,1)S(1)} %copy-done.2), kind=kOutput, calls=%fused_computation.41 | convolution fusion | flops 302063616 | bytes 2506752 | tf_op jit(solution)/shard_map/dot_general | solution.py:410
  117.8 0.7 convert_element_type.92.state_ref
  118.5 23.6 %shard_map.191 = (bf16[8,192,256]{2,1,0:T(8,128)(2,1)}, bf16[8,48,384]{2,1,0:T(8,128)(2,1)}) custom-call(bf16[8,192,256]{2,1,0:T(8,128)(2,1)} %bitcast.146, bf16[48,384]{1,0:T(8,128)(2,1)} %convert_element_type.92.state_ref), custom_call_target="tpu_custom_call" | custom-call | tf_op jit(solution)/shard_map/pallas_call | solution.py:318
  142.1 0.8 slice.52
  143.5 1.0 multiply_reduce_fusion
  146.0 0.8 copy.154
  148.2 0.7 copy.153
  149.0 1.1 fusion.33
  150.7 0.7 copy.152
  151.4 2.9 %convolution_bitcast_fusion.2 = f32[256,384]{1,0:T(8,128)} fusion(bf16[8,192,256]{2,1,0:T(8,128)(2,1)} %get-tuple-element.25, bf16[8,192,384]{2,1,0:T(8,128)(2,1)} %get-tuple-element.26), kind=kOutput, calls=%fused_computation.35 | convolution fusion | flops 301989888 | bytes 2359296 | tf_op jit(solution)/shard_map/dot_general | solution.py:437
  154.4 4.5 %fusion.2 = bf16[1,512,2048]{2,1,0:T(8,128)(2,1)} fusion(bf16[2,512,2048]{2,1,0:T(8,128)(2,1)} %get-tuple-element.24, f32[512,512]{1,0:T(8,128)S(1)} %copy-done.17, f32[512,512]{1,0:T(8,128)S(1)} %copy-done.15), kind=kOutput, calls=%fused_computation.6 | convolution fusion | flops 1076363264 | bytes 6291456 | tf_op jit(solution)/shard_map/dot_general | solution.py:346
  158.9 2.6 %fusion.1 = bf16[1,2048,512]{2,1,0:T(8,128)(2,1)} fusion(bf16[512,512]{1,0:T(8,128)(2,1)S(1)} %copy-done.6, bf16[2,512,2048]{2,1,0:T(8,128)(2,1)S(1)} %copy-done.12), kind=kOutput, calls=%fused_computation.5 | convolution fusion | flops 1074790400 | bytes 4718592 | tf_op jit(solution)/shard_map/dot_general | solution.py:348
  161.5 2.6 %fusion = bf16[1,2048,512]{2,1,0:T(8,128)(2,1)} fusion(bf16[512,512]{1,0:T(8,128)(2,1)S(1)} %copy-done.4, bf16[2,512,2048]{2,1,0:T(8,128)(2,1)S(1)} %copy-done.12), kind=kOutput, calls=%fused_computation.4 | convolution fusion | flops 1074790400 | bytes 4718592 | tf_op jit(solution)/shard_map/dot_general | solution.py:347
  (84 shorter events, 8.3 us)
Async XLA Ops:
  0.6 72.0 %copy-start = (bf16[1,2048,512]{2,1,0:T(8,128)(2,1)S(1)}, bf16[1,2048,512]{2,1,0:T(8,128)(2,1)}, u32[]{:S(2)}) copy-start(bf16[1,2048,512]{2,1,0:T(8,128)(2,1)} %param.20) | copy-start | bytes 6291460
  4.1 4.9 %copy-start.10 = (f32[192,4]{0,1:T(4,128)S(1)}, f32[192,4]{0,1:T(4,128)}, u32[]{:S(2)}) copy-start(f32[192,4]{0,1:T(4,128)} %param.28) | copy-start | bytes 9220
  72.6 3.0 %copy-start.1 = (bf16[1,2048,512]{2,1,0:T(8,128)(2,1)S(1)}, bf16[1,2048,512]{2,1,0:T(8,128)(2,1)}, u32[]{:S(2)}) copy-start(bf16[1,2048,512]{2,1,0:T(8,128)(2,1)} %param.21) | copy-start | bytes 6291460
  72.6 3.4 %copy-start.11 = (bf16[2,512,2048]{2,1,0:T(8,128)(2,1)S(1)}, bf16[2,512,2048]{2,1,0:T(8,128)(2,1)}, u32[]{:S(2)}) copy-start(bf16[2,512,2048]{2,1,0:T(8,128)(2,1)} %get-tuple-element.24) | copy-start | bytes 12582916
  76.1 1.3 copy-start.14
  76.1 2.0 %copy-start.13 = (bf16[1,512,2048]{2,1,0:T(8,128)(2,1)S(1)}, bf16[1,512,2048]{2,1,0:T(8,128)(2,1)}, u32[]{:S(2)}) copy-start(bf16[1,512,2048]{2,1,0:T(8,128)(2,1)} %param.22) | copy-start | bytes 6291460
  78.0 1.6 copy-start.16
  79.6 1.3 copy-start.3
  79.7 1.3 copy-start.5
  84.3 31.0 %copy-start.2 = (bf16[384,2048]{1,0:T(8,128)(2,1)S(1)}, bf16[384,2048]{1,0:T(8,128)(2,1)}, u32[]{:S(2)}) copy-start(bf16[384,2048]{1,0:T(8,128)(2,1)} %param.23) | copy-start | bytes 4718596
  113.2 4.2 %copy-start.8 = (bf16[192,192]{1,0:T(8,128)(2,1)S(1)}, bf16[192,192]{1,0:T(8,128)(2,1)}, u32[]{:S(2)}) copy-start(bf16[192,192]{1,0:T(8,128)(2,1)} %param.25) | copy-start | bytes 221188
  115.3 29.4 %copy-start.9 = (bf16[192,192]{1,0:T(8,128)(2,1)S(1)}, bf16[192,192]{1,0:T(8,128)(2,1)}, u32[]{:S(2)}) copy-start(bf16[192,192]{1,0:T(8,128)(2,1)} %param.26) | copy-start | bytes 221188
  144.7 2.1 %copy-start.7 = (bf16[192,384]{1,0:T(8,128)(2,1)S(1)}, bf16[192,384]{1,0:T(8,128)(2,1)}, u32[]{:S(2)}) copy-start(bf16[192,384]{1,0:T(8,128)(2,1)} %param.27) | copy-start | bytes 442372
  150.7 3.7 %copy-start.15 = (f32[512,512]{1,0:T(8,128)S(1)}, f32[512,512]{1,0:T(8,128)}, u32[]{:S(2)}) copy-start(f32[512,512]{1,0:T(8,128)} %copy-done.14) | copy-start | bytes 3145732
  151.4 3.0 %copy-start.17 = (f32[512,512]{1,0:T(8,128)S(1)}, f32[512,512]{1,0:T(8,128)}, u32[]{:S(2)}) copy-start(f32[512,512]{1,0:T(8,128)} %copy-done.16) | copy-start | bytes 3145732
  154.4 4.5 %copy-start.6 = (bf16[512,512]{1,0:T(8,128)(2,1)S(1)}, bf16[512,512]{1,0:T(8,128)(2,1)}, u32[]{:S(2)}) copy-start(bf16[512,512]{1,0:T(8,128)(2,1)} %copy-done.5) | copy-start | bytes 1572868
  154.4 4.5 %copy-start.12 = (bf16[2,512,2048]{2,1,0:T(8,128)(2,1)S(1)}, bf16[2,512,2048]{2,1,0:T(8,128)(2,1)}, u32[]{:S(2)}) copy-start(bf16[2,512,2048]{2,1,0:T(8,128)(2,1)} %get-tuple-element.24) | copy-start | bytes 12582916
  158.9 2.6 %copy-start.4 = (bf16[512,512]{1,0:T(8,128)(2,1)S(1)}, bf16[512,512]{1,0:T(8,128)(2,1)}, u32[]{:S(2)}) copy-start(bf16[512,512]{1,0:T(8,128)(2,1)} %copy-done.3) | copy-start | bytes 1572868

commit v2 on v1

--- a/solution.py
+++ b/solution.py
@@ -40,30 +40,53 @@
 
 
 def dispatch_kernel(
-    n, ny, send_ref, kept_ref, ends_ref, out_ref, kept_out, ends_out,
-    local_sem, a_send, a_recv, e_send, e_recv, y_send, y_recv, p_send, p_recv,
-    r_send, r_recv, l_send, l_recv, x_send, x_recv,
+    n, ny, cap, route_ref, decay_ref, rows_ref, grad_ref, out_ref, pick_ref, ends_out,
+    send_ref, local_sem, a_send, a_recv, e_send, e_recv, y_send, y_recv, p_send, p_recv,
 ):
     s, t, y, c = where_am_i(n, ny)
-    cap, q = send_ref.shape[2], send_ref.shape[3]
-    nz = n // 2
-    z, x = lax.div(s, 2), lax.rem(s, 2)
+    q = grad_ref.shape[1]
+    tokens, heads = decay_ref.shape
+    partner = (s, y * 2 + 1 - c)
+
+    ids = [route_ref[j : j + 1, :] for j in range(2)]
+    weights = [route_ref[j : j + 1, :] for j in range(2, 4)]
+    expert = lax.broadcasted_iota(jnp.int32, (n, tokens), 0).astype(F32)
+    named = [(expert == own).astype(F32) for own in ids]
+    first = lax.broadcasted_iota(jnp.int32, (tokens, tokens), 0)
+    second = lax.broadcasted_iota(jnp.int32, (tokens, tokens), 1)
+    earlier = jnp.dot(
+        (named[0] + named[1]).astype(BF16),
+        (first < second).astype(F32).astype(BF16),
+        preferred_element_type=F32,
+    )
+    slot = [
+        own * cap + jnp.sum(hot * earlier, axis=0, keepdims=True) for own, hot in zip(ids, named)
+    ]
+    number = lax.broadcasted_iota(jnp.int32, (n * cap, tokens), 0).astype(F32)
+    hits = [(number == own).astype(F32) for own in slot]
+    picker = (hits[0] + hits[1]).astype(BF16)
+    slot_weight = jnp.sum(hits[0] * weights[0] + hits[1] * weights[1], axis=1, keepdims=True)
+    pick_ref[...] = picker
+    ends_out[s, :, :] = jnp.zeros((8, 128), F32)
+    ends_out[s, :, pl.ds(0, heads)] = jnp.broadcast_to(
+        jnp.sum(decay_ref[...], axis=0, keepdims=True), (8, heads)
+    )
+    own_rows = rows_ref[:, pl.ds(pl.multiple_of(t * q, q), q)]
+    picked = jnp.dot(picker, own_rows, preferred_element_type=F32).astype(BF16)
+    send_ref[:, 0] = picked.reshape(n, cap, q)
+    cotangent = jnp.dot(picker, grad_ref[...], preferred_element_type=F32) * slot_weight
+    send_ref[:, 1] = cotangent.astype(BF16).reshape(n, cap, q)
+
     greet(sp_peers(n, s, t) + tp_peers(ny, s, y, c))
-    partner = (s, y * 2 + 1 - c)
 
     def block(src, tt):
         rows = pl.ds(pl.multiple_of(src * cap, cap), cap)
         columns = pl.ds(pl.multiple_of(tt * q, q), q)
         return out_ref.at[:, rows, columns]
 
-    own = [
-        pltpu.make_async_copy(send_ref.at[s], block(s, t), local_sem.at[0]),
-        pltpu.make_async_copy(kept_ref, kept_out.at[s], local_sem.at[1]),
-        pltpu.make_async_copy(ends_ref, ends_out.at[s], local_sem.at[2]),
-    ]
-    for copy in own:
-        copy.start()
-    arrivals, waits = [own[0]], []
+    own = pltpu.make_async_copy(send_ref.at[s], block(s, t), local_sem.at[0])
+    own.start()
+    arrivals, waits = [own], []
     for k in range(1, n):
         peer = lax.rem(s + k, n)
         copy = remote(send_ref.at[peer], block(s, t), a_send.at[k], a_recv.at[k], (peer, t))
@@ -72,31 +95,9 @@
         waits.append(copy.wait_send)
     for k in range(1, n):
         peer = lax.rem(s + k, n)
-        copy = remote(ends_ref, ends_out.at[s], e_send.at[k], e_recv.at[k], (peer, t))
+        copy = remote(ends_out.at[s], ends_out.at[s], e_send.at[k], e_recv.at[k], (peer, t))
         copy.start()
         waits.append(copy.wait)
-
-    def at(zz):
-        return lax.rem(zz + 2 * nz, nz) * 2 + x
-
-    def hop(j, sign, send, recv, source):
-        held = at(z - sign * j)
-        copy = remote(source, kept_out.at[held], send.at[j], recv.at[j], (at(z + sign), t))
-        copy.start()
-        waits.append(copy.wait_send)
-        return copy
-
-    right_steps, left_steps = nz // 2, nz - 1 - nz // 2
-    right = hop(0, 1, r_send, r_recv, kept_ref) if right_steps else None
-    left = hop(0, -1, l_send, l_recv, kept_ref) if left_steps else None
-    pair = (z * 2 + 1 - x, t)
-
-    def across(held, index, source):
-        copy = remote(source, kept_out.at[held], x_send.at[index], x_recv.at[index], pair)
-        copy.start()
-        waits.append(copy.wait)
-
-    across(s, 0, kept_ref)
     from_far = {}
     for k in range(n + 1):
         if k < n:
@@ -123,51 +124,36 @@
                 copy = remote(theirs, theirs, p_send.at[d, k - 1], p_recv.at[d, k - 1], partner)
                 copy.start()
                 waits.append(copy.wait)
-    index = 1
-    for j in range(1, right_steps + 1):
-        right.wait_recv()
-        held = at(z - j)
-        if j < right_steps:
-            right = hop(j, 1, r_send, r_recv, kept_out.at[held])
-        across(held, index, kept_out.at[held])
-        index += 1
-        if j <= left_steps:
-            left.wait_recv()
-            held = at(z + j)
-            if j < left_steps:
-                left = hop(j, -1, l_send, l_recv, kept_out.at[held])
-            across(held, index, kept_out.at[held])
-            index += 1
-    own[1].wait()
-    own[2].wait()
     for wait in waits:
         wait()
 
 
-def dispatch(n, ny, send, kept, ends):
-    cap, q = send.shape[2], send.shape[3]
+def dispatch(n, ny, cap, route, decay, rows, grad):
+    tokens, q = grad.shape
     dma = pltpu.SemaphoreType.DMA
     return pl.pallas_call(
-        functools.partial(dispatch_kernel, n, ny),
+        functools.partial(dispatch_kernel, n, ny, cap),
         out_shape=(
             jax.ShapeDtypeStruct((2, n * cap, q * ny * 2), BF16),
-            jax.ShapeDtypeStruct((n,) + kept.shape, BF16),
-            jax.ShapeDtypeStruct((n,) + ends.shape, F32),
-        ),
-        in_specs=[pl.BlockSpec(memory_space=pltpu.VMEM)] * 3,
+            jax.ShapeDtypeStruct((n * cap, tokens), BF16),
+            jax.ShapeDtypeStruct((n, 8, 128), F32),
+        ),
+        in_specs=[pl.BlockSpec(memory_space=pltpu.VMEM)] * 4,
         out_specs=[pl.BlockSpec(memory_space=pltpu.VMEM)] * 3,
-        scratch_shapes=[dma((3,)), dma((n,)), dma((n,)), dma((n,)), dma((n,))]
-        + [dma((ny, n))] * 4
-        + [dma((n,))] * 6,
+        scratch_shapes=[pltpu.VMEM((n, 2, cap, q), BF16)]
+        + [dma((1,)), dma((n,)), dma((n,)), dma((n,)), dma((n,))]
+        + [dma((ny, n))] * 4,
         compiler_params=pltpu.CompilerParams(
             collective_id=0, has_side_effects=True, vmem_limit_bytes=LIMIT
         ),
-    )(send, kept, ends)
+    )(route, decay, rows, grad)
 
 
 def combine_kernel(
-    n, ny, part_ref, pick_ref, grad_ref, stream_ref, near, pairs, far, share, back,
+    n, ny, part_ref, pick_ref, grad_ref, kept_ref, stream_ref, blocks_ref, kept_out,
+    near, pairs, far, share, back,
     p_send, p_recv, y_send, y_recv, a_send, a_recv, g_send, g_recv, h_send, h_recv,
+    local_sem, r_send, r_recv, l_send, l_recv, x_send, x_recv,
 ):
     s, t, y, c = where_am_i(n, ny)
     q = grad_ref.shape[1]
@@ -182,6 +168,45 @@
     def rows(b):
         return pl.ds(pl.multiple_of(b * cap, cap), cap)
 
+    nz = n // 2
+    z, x = lax.div(s, 2), lax.rem(s, 2)
+    pair = (z * 2 + 1 - x, t)
+    kept_own = pltpu.make_async_copy(kept_ref, kept_out.at[s], local_sem.at[0])
+    kept_own.start()
+    waits.append(kept_own.wait)
+
+    def at(zz):
+        return lax.rem(zz + 2 * nz, nz) * 2 + x
+
+    def hop(j, sign, send, recv, source):
+        held = at(z - sign * j)
+        copy = remote(source, kept_out.at[held], send.at[j], recv.at[j], (at(z + sign), t))
+        copy.start()
+        waits.append(copy.wait_send)
+        return copy
+
+    def across(held, index, source):
+        copy = remote(source, kept_out.at[held], x_send.at[index], x_recv.at[index], pair)
+        copy.start()
+        waits.append(copy.wait)
+
+    right_steps, left_steps = nz // 2, nz - 1 - nz // 2
+    moving = {}
+
+    def relay(j):
+        if j <= right_steps:
+            moving["right"].wait_recv()
+            held = at(z - j)
+            if j < right_steps:
+                moving["right"] = hop(j, 1, r_send, r_recv, kept_out.at[held])
+            across(held, 2 * j - 1, kept_out.at[held])
+        if j <= left_steps:
+            moving["left"].wait_recv()
+            held = at(z + j)
+            if j < left_steps:
+                moving["left"] = hop(j, -1, l_send, l_recv, kept_out.at[held])
+            across(held, 2 * j, kept_out.at[held])
+
     halves = {}
     for d in list(range(1, ny)) + [0]:
         theirs = lax.rem(y + d, ny) * 2 + 1 - c
@@ -191,6 +216,11 @@
         copy.start()
         waits.append(copy.wait_send)
         halves[d] = copy
+    if right_steps:
+        moving["right"] = hop(0, 1, r_send, r_recv, kept_ref)
+    if left_steps:
+        moving["left"] = hop(0, -1, l_send, l_recv, kept_ref)
+    across(s, 0, kept_ref)
     arrived = {}
     for d in range(1, ny):
         halves[d].wait_recv()
@@ -228,9 +258,13 @@
             returns.append(copy)
         else:
             back[b, :] = total.astype(BF16)
+        if k % 2 == 0:
+            relay(k // 2)
     for copy in returns:
         copy.wait_recv()
-    token = jnp.dot(pick_ref[...], back[...], preferred_element_type=F32)
+    token = lax.dot_general(
+        pick_ref[...], back[...], (((0,), (0,)), ((), ())), preferred_element_type=F32
+    )
     stream_ref[:, columns(t)] = (grad_ref[...].astype(F32) + token).astype(BF16)
     mine = stream_ref.at[:, columns(t)]
     outer = []
@@ -252,26 +286,35 @@
         waits.append(copy.wait)
     for wait in waits:
         wait()
-
-
-def combine(n, ny, part, pick, grad):
+    wide = blocks_ref.shape[2]
+    for b in range(n):
+        blocks_ref[b] = stream_ref[:, b * wide : (b + 1) * wide]
+
+
+def combine(n, ny, part, pick, grad, kept):
     slots, q = part.shape[0], grad.shape[1]
     dma = pltpu.SemaphoreType.DMA
     return pl.pallas_call(
         functools.partial(combine_kernel, n, ny),
-        out_shape=jax.ShapeDtypeStruct((grad.shape[0], q * ny * 2), BF16),
-        in_specs=[pl.BlockSpec(memory_space=pltpu.VMEM)] * 3,
-        out_specs=pl.BlockSpec(memory_space=pltpu.VMEM),
+        out_shape=(
+            jax.ShapeDtypeStruct((grad.shape[0], q * ny * 2), BF16),
+            jax.ShapeDtypeStruct((n, grad.shape[0], q * ny * 2 // n), BF16),
+            jax.ShapeDtypeStruct((n,) + kept.shape, BF16),
+        ),
+        in_specs=[pl.BlockSpec(memory_space=pltpu.VMEM)] * 4,
+        out_specs=[pl.BlockSpec(memory_space=pltpu.VMEM)] * 3,
         scratch_shapes=[pltpu.VMEM((ny, slots, q), BF16)] * 3
         + [pltpu.VMEM((slots, q), BF16)] * 2
         + [dma((ny,))] * 2
         + [dma((ny, n))] * 2
         + [dma((n,))] * 2
-        + [dma((ny,))] * 4,
+        + [dma((ny,))] * 4
+        + [dma((1,))]
+        + [dma((n,))] * 6,
         compiler_params=pltpu.CompilerParams(
             collective_id=1, has_side_effects=True, vmem_limit_bytes=LIMIT
         ),
-    )(part, pick, grad)
+    )(part, pick, grad, kept)
 
 
 def tail_kernel(
@@ -372,41 +415,24 @@
     bf16 = jnp.bfloat16
     upper_limit = lax.Precision.HIGHEST
     tokens_here = moe_input.shape[0]
-    width = moe_input.shape[1]
     sp_count = lax.axis_size("sp")
     tp_count = lax.axis_size("tp")
     capacity = -(-(5 * tokens_here // (2 * sp_count)) // 16) * 16
-    slot_count = sp_count * capacity
-    flat_ids = expert_ids.reshape(-1)
-    flat_weights = expert_weights.reshape(-1)
-    onehot = (flat_ids[:, None] == jnp.arange(sp_count, dtype=jnp.int32)[None, :]).astype(jnp.int32)
-    ranks = jnp.sum((jnp.cumsum(onehot, axis=0) - onehot) * onehot, axis=1)
-    slot_of = flat_ids * capacity + ranks
-    hits = jnp.arange(slot_count, dtype=jnp.int32)[:, None] == slot_of[None, :]
-    picker = jnp.any(hits.reshape(slot_count, tokens_here, 2), axis=2).astype(bf16)
-    slot_weight = jnp.sum(jnp.where(hits, flat_weights[None, :], 0.0), axis=1)
     along = (((0,), (0,)), ((), ()))
-    column_count = width // tp_count
     ny = tp_count // 2
     heads_here = log_decay.shape[1]
     running_total = jnp.cumsum(log_decay, axis=0)
     last_sum = running_total[-1]
-    own_rows = lax.dynamic_slice_in_dim(
-        moe_input, lax.axis_index("tp") * column_count, column_count, 1
-    )
-    send_rows = jnp.dot(picker, own_rows, preferred_element_type=f32).astype(bf16)
-    send_grad = (
-        jnp.dot(picker, out_grad, preferred_element_type=f32) * slot_weight[:, None]
-    ).astype(bf16)
-    send = jnp.stack(
-        [part.reshape(sp_count, capacity, column_count) for part in (send_rows, send_grad)], axis=1
-    )
-    ends = jnp.zeros((8, 128), f32).at[:, :heads_here].set(last_sum[None, :])
-    received, kept_all, ends_all = dispatch(sp_count, ny, send, retained, ends)
+    route = jnp.concatenate([expert_ids.astype(f32).T, expert_weights.T], axis=0)
+    received, picker, ends_all = dispatch(
+        sp_count, ny, capacity, route, log_decay, moe_input, out_grad
+    )
     gate_w_grad, up_w_grad, down_grad, partial_value = expert_back(
         received[0], received[1], w_gate[0], w_up[0], w_down[0]
     )
-    stream = combine(sp_count, ny, partial_value.astype(bf16), picker.T, out_grad)
+    stream, stream_blocks, kept_all = combine(
+        sp_count, ny, partial_value.astype(bf16), picker, out_grad, retained
+    )
     ret_grad = lax.dot_general(
         stream, out_proj, (((1,), (1,)), ((), ())), preferred_element_type=f32
     ).astype(bf16)
@@ -432,7 +458,6 @@
         precision=upper_limit,
     )
     flat_state = added_input.transpose(1, 0, 2).reshape(key_dim, heads_here * value_dim)
-    stream_blocks = stream.reshape(tokens_here, sp_count, width // sp_count).transpose(1, 0, 2)
     stream_all, states = tail_exchange(sp_count, ny, stream_blocks, flat_state.astype(bf16))
     out_proj_grad = lax.dot_general(
         stream_all.reshape(sp_count * tokens_here, -1),

time: 166 us -> 151 us (0.910)
  Pallas kernels: 112 us -> 108 us
  local copies, waits for them, and re-layouts: 11.7 us -> 8.04 us
  other arithmetic: 7.89 us -> 4.81 us
  matrix products: 31.2 us -> 28.5 us
    another operation x7 -> x2, other arithmetic: 4.51 us -> 1.26 us
    dot_general x2 -> x0, matrix products: 2.56 us -> none  [the longest x1 1.28 us: on_device(): jnp.dot(picker, out_grad, preferred_element_type=f32) * slot_weight[:, None]]
    pallas_call x2, Pallas kernels: 88.8 us -> 86.6 us  [the longest x1 43.5 us: combine(): pl.pallas_call(functools.partial(combine_kernel, n, ny), out_shape=(jax.S...]
    pallas_call x1, Pallas kernels: 23.6 us -> 21.4 us  [tail_exchange(): pl.pallas_call(functools.partial(tail_kernel, n, ny), out_shape=(jax.Shap...]
    reshape x1, local copies, waits for them, and re-layouts: 2.1 us -> 0.01 us  [on_device(): stream.reshape(tokens_here, sp_count, width // sp_count).transpose(1, 0, 2)]
    dot_general x1, matrix products: 4.48 us -> 2.71 us  [expert_back(): lax.dot_general(act, grad, along, preferred_element_type=f32).astype(bf16)]
    dot_general x1, matrix products: 2.63 us -> 4.35 us  [expert_back(): lax.dot_general(rows, up_grad, along, preferred_element_type=f32)]
    unnamed x44 -> x43, local copies, waits for them, and re-layouts: 5.45 us -> 5.33 us
where the time goes in v2:
time: 151 us; the launch traced here: 150 us
  Pallas kernels  108 us (72%)
  matrix products  28.5 us (19%)
  local copies, waits for them, and re-layouts  8.04 us (5%)
  other arithmetic  4.81 us (3%)
    pallas_call x1, Pallas kernels, combine(): pl.pallas_call(functools.partial(combine_kernel, n, ny), out_shape=(jax.S...  43.5 us
    pallas_call x1, Pallas kernels, dispatch(): pl.pallas_call(functools.partial(dispatch_kernel, n, ny, cap), out_shape=...  43 us
    pallas_call x1, Pallas kernels, tail_exchange(): pl.pallas_call(functools.partial(tail_kernel, n, ny), out_shape=(jax.Shap...  21.4 us
    unnamed x43, local copies, waits for them, and re-layouts  5.33 us
    dot_general x1, matrix products, expert_back(): lax.dot_general(rows, up_grad, along, preferred_element_type=f32)  4.35 us

profile of v2, /device:TPU:0, one launch (start us, length us, event | category | flops | bytes accessed | tf_op | source)
XLA Modules:
  0.0 150.3 jit_solution(13631144776751140248)
XLA Ops:
  0.6 1.6 %copy.90.decay_ref = f32[192,4]{1,0:T(8,128)} copy(f32[192,4]{0,1:T(4,128)} %param.26) | data formatting | bytes 6144 | tf_op args[12]
  2.2 0.7 convert_bitcast_fusion
  2.9 1.3 pad_maximum_fusion.route_ref
  4.2 43.0 %shard_map.189 = (bf16[2,512,2048]{2,1,0:T(8,128)(2,1)}, bf16[512,192]{1,0:T(8,128)(2,1)}, f32[8,8,128]{2,1,0:T(8,128)}) custom-call(f32[4,192]{1,0:T(4,128)} %pad_maximum_fusion.route_ref, f32[192,4]{1,0:T(8,128)} %copy.90.decay_ref, bf16[192,2048]{1,0:T(8,128)(2,1)} %rows_ref.1, bf16[192,512]{1,0:T(8,128)(2,1)} %grad_ref.3), custom_call_target="tpu_custom_call" | custom-call | tf_op jit(solution)/shard_map/pallas_call | solution.py:134
  47.3 3.0 %fusion.5 = f32[512,512]{1,0:T(8,128)S(1)} fusion(bf16[1,2048,512]{2,1,0:T(8,128)(2,1)S(1)} %copy-done, bf16[2,512,2048]{2,1,0:T(8,128)(2,1)} %get-tuple-element.15), kind=kOutput, calls=%fused_computation.9 | convolution fusion | flops 1073741824 | bytes 5242880 | tf_op jit(solution)/shard_map/dot_general | solution.py:379
  50.3 0.4 copy-done.11
  50.7 1.2 fusion.8
  52.0 0.7 copy-done.13
  52.7 1.6 %multiply_convert_fusion.1 = (bf16[512,512]{1,0:T(8,128)(2,1)S(1)}, bf16[512,512]{1,0:T(8,128)(2,1)S(1)}) fusion(f32[512,512]{1,0:T(8,128)S(1)} %fusion.5, f32[512,512]{1,0:T(8,128)S(1)} %fusion.8, bf16[1,512,2048]{2,1,0:T(8,128)(2,1)S(1)} %copy-done.13, bf16[2,512,2048]{2,1,0:T(8,128)(2,1)S(1)} %copy-done.11), kind=kOutput, calls=%fused_computation.52 | convolution fusion | flops 1077149696 | bytes 7340032 | tf_op jit(solution)/shard_map/dot_general | solution.py:386
  54.3 1.3 fusion.3
  55.7 2.6 %add_convert_fusion.part_ref = bf16[512,2048]{1,0:T(8,128)(2,1)} fusion(f32[512,2048]{1,0:T(8,128)S(1)} %fusion.3, bf16[512,512]{1,0:T(8,128)(2,1)S(1)} %get-tuple-element.51, bf16[1,2048,512]{2,1,0:T(8,128)(2,1)S(1)} %copy-done.1), kind=kOutput, calls=%fused_computation | convolution fusion | flops 1075838976 | bytes 8912896 | tf_op jit(solution)/shard_map/dot_general | solution.py:394
  58.3 43.5 %shard_map.190 = (bf16[192,2048]{1,0:T(8,128)(2,1)}, bf16[8,192,256]{2,1,0:T(8,128)(2,1)}, bf16[8,192,384]{2,1,0:T(8,128)(2,1)}) custom-call(bf16[512,2048]{1,0:T(8,128)(2,1)} %add_convert_fusion.part_ref, bf16[512,192]{1,0:T(8,128)(2,1)} %get-tuple-element.16.pick_ref, bf16[192,512]{1,0:T(8,128)(2,1)} %grad_ref.3, bf16[192,384]{1,0:T(8,128)(2,1)} %kept_ref.1), custom_call_target="tpu_custom_call" | custom-call | tf_op jit(solution)/shard_map/pallas_call | solution.py:297
  101.9 1.8 %convolution_convert_fusion.3 = bf16[192,384]{1,0:T(8,128)(2,1)S(1)} fusion(bf16[192,2048]{1,0:T(8,128)(2,1)} %get-tuple-element.18, bf16[384,2048]{1,0:T(8,128)(2,1)S(1)} %copy-done.2), kind=kOutput, calls=%fused_computation.38 | convolution fusion | flops 302063616 | bytes 2506752 | tf_op jit(solution)/shard_map/dot_general | solution.py:436
  103.9 1.2 reduce-window.6
  106.2 0.7 convert_element_type.70.state_ref
  107.0 21.4 %shard_map.191 = (bf16[8,192,256]{2,1,0:T(8,128)(2,1)}, bf16[8,48,384]{2,1,0:T(8,128)(2,1)}) custom-call(bf16[8,192,256]{2,1,0:T(8,128)(2,1)} %get-tuple-element.17.stream_ref, bf16[48,384]{1,0:T(8,128)(2,1)} %convert_element_type.70.state_ref), custom_call_target="tpu_custom_call" | custom-call | tf_op jit(solution)/shard_map/pallas_call | solution.py:361
  128.3 0.8 slice.28
  129.8 1.0 multiply_reduce_fusion
  131.1 0.4 fusion.24
  131.5 0.4 convolution_bitcast_fusion.4
  131.9 0.4 fusion.28
  132.3 0.8 copy.109
  133.3 0.5 fusion.31
  134.1 0.4 fusion.34
  134.5 0.7 copy.108
  135.3 1.1 fusion.32
  136.4 0.5 fusion.33
  137.0 0.7 copy.107
  137.7 2.9 %convolution_bitcast_fusion.2 = f32[256,384]{1,0:T(8,128)} fusion(bf16[8,192,256]{2,1,0:T(8,128)(2,1)} %get-tuple-element.19, bf16[8,192,384]{2,1,0:T(8,128)(2,1)} %get-tuple-element.20), kind=kOutput, calls=%fused_computation.32 | convolution fusion | flops 301989888 | bytes 2359296 | tf_op jit(solution)/shard_map/dot_general | solution.py:462
  140.6 4.4 %fusion.1 = bf16[1,2048,512]{2,1,0:T(8,128)(2,1)} fusion(bf16[512,512]{1,0:T(8,128)(2,1)S(1)} %copy-done.6, bf16[2,512,2048]{2,1,0:T(8,128)(2,1)} %get-tuple-element.15), kind=kOutput, calls=%fused_computation.5 | convolution fusion | flops 1074790400 | bytes 4718592 | tf_op jit(solution)/shard_map/dot_general | solution.py:391
  144.9 2.6 %fusion = bf16[1,2048,512]{2,1,0:T(8,128)(2,1)} fusion(bf16[512,512]{1,0:T(8,128)(2,1)S(1)} %copy-done.4, bf16[2,512,2048]{2,1,0:T(8,128)(2,1)S(1)} %copy-done.12), kind=kOutput, calls=%fused_computation.4 | convolution fusion | flops 1074790400 | bytes 4718592 | tf_op jit(solution)/shard_map/dot_general | solution.py:390
  147.6 2.7 %fusion.2 = bf16[1,512,2048]{2,1,0:T(8,128)(2,1)} fusion(bf16[2,512,2048]{2,1,0:T(8,128)(2,1)S(1)} %copy-done.12, f32[512,512]{1,0:T(8,128)S(1)} %copy-done.17, f32[512,512]{1,0:T(8,128)S(1)} %copy-done.15), kind=kOutput, calls=%fused_computation.6 | convolution fusion | flops 1076363264 | bytes 6291456 | tf_op jit(solution)/shard_map/dot_general | solution.py:389
  (62 shorter events, 2.8 us)
Async XLA Ops:
  0.6 46.6 %copy-start = (bf16[1,2048,512]{2,1,0:T(8,128)(2,1)S(1)}, bf16[1,2048,512]{2,1,0:T(8,128)(2,1)}, u32[]{:S(2)}) copy-start(bf16[1,2048,512]{2,1,0:T(8,128)(2,1)} %param.18) | copy-start | bytes 6291460
  47.3 3.0 %copy-start.1 = (bf16[1,2048,512]{2,1,0:T(8,128)(2,1)S(1)}, bf16[1,2048,512]{2,1,0:T(8,128)(2,1)}, u32[]{:S(2)}) copy-start(bf16[1,2048,512]{2,1,0:T(8,128)(2,1)} %param.19) | copy-start | bytes 6291460
  47.3 3.4 %copy-start.11 = (bf16[2,512,2048]{2,1,0:T(8,128)(2,1)S(1)}, bf16[2,512,2048]{2,1,0:T(8,128)(2,1)}, u32[]{:S(2)}) copy-start(bf16[2,512,2048]{2,1,0:T(8,128)(2,1)} %get-tuple-element.15) | copy-start | bytes 12582916
  50.7 1.3 copy-start.14
  50.7 2.0 %copy-start.13 = (bf16[1,512,2048]{2,1,0:T(8,128)(2,1)S(1)}, bf16[1,512,2048]{2,1,0:T(8,128)(2,1)}, u32[]{:S(2)}) copy-start(bf16[1,512,2048]{2,1,0:T(8,128)(2,1)} %param.20) | copy-start | bytes 6291460
  52.7 1.6 %copy-start.16 = (f32[512,512]{1,0:T(8,128)}, f32[512,512]{1,0:T(8,128)S(1)}, u32[]{:S(2)}) copy-start(f32[512,512]{1,0:T(8,128)S(1)} %fusion.8) | copy-start | bytes 3145732
  54.3 1.3 copy-start.3
  54.3 1.3 copy-start.5
  58.3 43.6 %copy-start.2 = (bf16[384,2048]{1,0:T(8,128)(2,1)S(1)}, bf16[384,2048]{1,0:T(8,128)(2,1)}, u32[]{:S(2)}) copy-start(bf16[384,2048]{1,0:T(8,128)(2,1)} %param.21) | copy-start | bytes 4718596
  101.8 2.0 %copy-start.10 = (f32[192,4]{0,1:T(4,128)S(1)}, f32[192,4]{0,1:T(4,128)}, u32[]{:S(2)}) copy-start(f32[192,4]{0,1:T(4,128)} %param.26) | copy-start | bytes 9220
  101.8 4.0 %copy-start.8 = (bf16[192,192]{1,0:T(8,128)(2,1)S(1)}, bf16[192,192]{1,0:T(8,128)(2,1)}, u32[]{:S(2)}) copy-start(bf16[192,192]{1,0:T(8,128)(2,1)} %param.23) | copy-start | bytes 221188
  101.8 29.1 %copy-start.9 = (bf16[192,192]{1,0:T(8,128)(2,1)S(1)}, bf16[192,192]{1,0:T(8,128)(2,1)}, u32[]{:S(2)}) copy-start(bf16[192,192]{1,0:T(8,128)(2,1)} %param.24) | copy-start | bytes 221188
  131.0 2.1 %copy-start.7 = (bf16[192,384]{1,0:T(8,128)(2,1)S(1)}, bf16[192,384]{1,0:T(8,128)(2,1)}, u32[]{:S(2)}) copy-start(bf16[192,384]{1,0:T(8,128)(2,1)} %param.25) | copy-start | bytes 442372
  136.9 3.6 %copy-start.6 = (bf16[512,512]{1,0:T(8,128)(2,1)S(1)}, bf16[512,512]{1,0:T(8,128)(2,1)}, u32[]{:S(2)}) copy-start(bf16[512,512]{1,0:T(8,128)(2,1)} %copy-done.5) | copy-start | bytes 1572868
  140.6 4.4 %copy-start.4 = (bf16[512,512]{1,0:T(8,128)(2,1)S(1)}, bf16[512,512]{1,0:T(8,128)(2,1)}, u32[]{:S(2)}) copy-start(bf16[512,512]{1,0:T(8,128)(2,1)} %copy-done.3) | copy-start | bytes 1572868
  140.6 4.4 %copy-start.12 = (bf16[2,512,2048]{2,1,0:T(8,128)(2,1)S(1)}, bf16[2,512,2048]{2,1,0:T(8,128)(2,1)}, u32[]{:S(2)}) copy-start(bf16[2,512,2048]{2,1,0:T(8,128)(2,1)} %get-tuple-element.15) | copy-start | bytes 12582916
  144.9 2.7 %copy-start.15 = (f32[512,512]{1,0:T(8,128)S(1)}, f32[512,512]{1,0:T(8,128)}, u32[]{:S(2)}) copy-start(f32[512,512]{1,0:T(8,128)} %copy-done.14) | copy-start | bytes 3145732
  144.9 2.7 %copy-start.17 = (f32[512,512]{1,0:T(8,128)S(1)}, f32[512,512]{1,0:T(8,128)}, u32[]{:S(2)}) copy-start(f32[512,512]{1,0:T(8,128)} %copy-done.16) | copy-start | bytes 3145732
